TPU v7x, 32 devices: a whole 2x2x4 slice. The times are simulated.
32 devices in a mesh: sp: 8 (over z, core), tp: 4 (over y, x).
Axes of the slice: x: 2, y: 2, z: 4, core: 2. Of those that a mesh axis runs over, the one named last changes fastest.
Arguments:
- moe_input: bfloat16 [1024, 2048], P('sp', 'tp'), may hold values from -6 to 6
- cotangent: bfloat16 [1024, 2048], P('sp', 'tp'), may hold values from -6 to 6
- routes: int32 [1024, 2], P('sp'), may hold values from 0 to 7, all different within a row; in each aligned block of 128 rows (0 to 127, 128 to 255, ...) at most 40 rows name the same one
- route_weights: float32 [1024, 2], P('sp'), may hold values from 0.2 to 1
- gate_branch: bfloat16 [1024, 2560], P('sp', 'tp'), may hold values from -6 to 6
- log_decay: float32 [1024, 2560], P('sp', 'tp'), may hold values from -0.12 to 0
- states: float32 [1024, 2560], P('sp', 'tp'), may hold values from -6 to 6
- w_gate: bfloat16 [8, 2048, 2048], P('sp', None, 'tp'), may hold values from -0.125 to 0.125
- w_up: bfloat16 [8, 2048, 2048], P('sp', None, 'tp'), may hold values from -0.125 to 0.125
- w_down: bfloat16 [8, 2048, 2048], P('sp', 'tp'), may hold values from -0.125 to 0.125
- out_proj: bfloat16 [2048, 2560], P('sp', 'tp'), may hold values from -0.125 to 0.125
Outputs:
- grad_w_gate: float32 [8, 2048, 2048], P('sp', None, 'tp')
- grad_w_up: float32 [8, 2048, 2048], P('sp', None, 'tp')
- grad_w_down: float32 [8, 2048, 2048], P('sp', 'tp')
- grad_out_proj: float32 [2048, 2560], P('sp', 'tp')
- grad_gate_branch: bfloat16 [1024, 2560], P('sp', 'tp')
- grad_log_decay: bfloat16 [1024, 2560], P('sp', 'tp')
- grad_input_term: float32 [1024, 2560], P('sp', 'tp')
Inputs may be any that keep to these rules, and one draw needn't show every extreme that they name: `routes`: in the rows of one device no expert is named by more than 40 entries, and in every draw some expert is named by exactly 40 entries of one device's rows.
All inputs are finite; a program needn't handle non-finite values.
Results may differ from a plain program's by a relative error of at most 0.025.
Values may be sent and summed in bfloat16 or wider, within the bound.
A program may use at most 64 MiB of HBM per device.

v0:
```python
import jax
import jax.numpy as jnp
from jax import lax
from jax.sharding import PartitionSpec as P


def carried_in(value, axis, join, neutral):
    count, mine = (lax.axis_size(axis), lax.axis_index(axis))
    pieces = jax.tree.map(lambda part: lax.all_gather(part, axis), value)
    pieces = jax.tree.map(lambda part: part[::-1], pieces)
    mine = count - 1 - mine
    subtotal = jax.tree.map(
        lambda part, zero: jnp.full_like(part, 0) + jnp.asarray(zero, part.dtype), value, neutral
    )

    def turn(position, subtotal):
        longer = join(subtotal, jax.tree.map(lambda part: part[position], pieces))
        return jax.tree.map(lambda new, old: jnp.where(position < mine, new, old), longer, subtotal)

    return lax.fori_loop(0, count - 1, turn, subtotal)


def from_behind(value, axis, steps):
    count = lax.axis_size(axis)
    leading, last = (max(0, -steps), min(count, count - steps))
    return lax.ppermute(value, axis, [(source, source + steps) for source in range(leading, last)])


def silu_parts(pre_gate):
    sigmoid_val = jax.nn.sigmoid(pre_gate)
    return (pre_gate * sigmoid_val, sigmoid_val * (1.0 + pre_gate * (1.0 - sigmoid_val)))


def combine_pair(left_pair, right_pair):
    return (left_pair[0] * right_pair[0], right_pair[0] * left_pair[1] + right_pair[1])


def compose_maps(earlier, later_map):
    return (earlier[0] * later_map[0], later_map[1] + later_map[0] * earlier[1])


def contract_rows(left_mat, right_mat):
    return lax.dot_general(
        left_mat, right_mat, (((0,), (0,)), ((), ())), preferred_element_type=jnp.float32
    )


def contract_cols(left_mat, right_mat):
    return lax.dot_general(
        left_mat, right_mat, (((1,), (1,)), ((), ())), preferred_element_type=jnp.float32
    )


def shards(
    moe_input,
    cotangent,
    routes,
    route_weights,
    gate_branch,
    log_decay,
    states,
    w_gate,
    w_up,
    w_down,
    out_proj,
):
    groups = lax.axis_size("sp")
    tok_rows, picks = routes.shape
    col_width = moe_input.shape[1]
    model_width = col_width * lax.axis_size("tp")
    room = tok_rows * picks * 5 // (4 * groups)
    flat_routes = routes.reshape(-1)
    onehot = (flat_routes[:, None] == jnp.arange(groups, dtype=jnp.int32)[None, :]).astype(
        jnp.int32
    )
    before = jnp.cumsum(onehot, axis=0) - onehot
    slot_index = jnp.sum(before * onehot, axis=1)
    target = flat_routes * room + slot_index
    owners = jnp.arange(tok_rows * picks, dtype=jnp.int32) // picks
    source = jnp.zeros((groups * room,), jnp.int32).at[target].set(owners)
    live_slot = jnp.zeros((groups * room,), jnp.bool_).at[target].set(True)
    slot_weight = jnp.zeros((groups * room,), jnp.float32).at[target].set(route_weights.reshape(-1))
    send_data = jnp.where(live_slot[:, None], moe_input[source], jnp.zeros((), jnp.bfloat16))
    send_cot = (slot_weight[:, None] * cotangent[source].astype(jnp.float32)).astype(jnp.bfloat16)
    part_rows, part_cot = (
        lax.all_to_all(
            send_data.reshape(groups, room, col_width),
            "sp",
            split_axis=0,
            concat_axis=0,
            tiled=True,
        ),
        lax.all_to_all(
            send_cot.reshape(groups, room, col_width), "sp", split_axis=0, concat_axis=0, tiled=True
        ),
    )
    rows_in, cot_in = (
        lax.all_gather(part_rows, "tp", axis=2, tiled=True),
        lax.all_gather(part_cot, "tp", axis=2, tiled=True),
    )
    row_data = rows_in.reshape(groups * room, model_width)
    scaled = cot_in.reshape(groups * room, model_width)
    gate_w = w_gate[0]
    up_w = w_up[0]
    down_w = w_down[0]
    pre_gate = jnp.dot(row_data, gate_w, preferred_element_type=jnp.float32)
    pre_up = jnp.dot(row_data, up_w, preferred_element_type=jnp.float32)
    active, slope = silu_parts(pre_gate)
    hidden = (active * pre_up).astype(jnp.bfloat16)
    grad_down = contract_rows(hidden, scaled)
    grad_hidden = contract_cols(scaled, down_w)
    grad_pre_gate = (grad_hidden * pre_up * slope).astype(jnp.bfloat16)
    grad_pre_up = (grad_hidden * active).astype(jnp.bfloat16)
    grad_gate_w = contract_rows(row_data, grad_pre_gate)
    grad_up_w = contract_rows(row_data, grad_pre_up)
    joined_grads = jnp.concatenate([grad_pre_gate, grad_pre_up], axis=1)
    joined_weights = jnp.concatenate([gate_w, up_w], axis=1)
    entry_terms = contract_cols(joined_grads, joined_weights)
    summed = lax.psum_scatter(
        entry_terms.reshape(groups, room, model_width).astype(jnp.bfloat16),
        "tp",
        scatter_dimension=2,
        tiled=True,
    )
    returned = lax.all_to_all(summed, "sp", split_axis=0, concat_axis=0, tiled=True)
    back_rows = returned.reshape(groups * room, col_width)[target].astype(jnp.float32)
    grad_cols = (
        jnp.sum(back_rows.reshape(tok_rows, picks, col_width), axis=1)
        + cotangent.astype(jnp.float32)
    ).astype(jnp.bfloat16)
    grad_tokens = lax.all_gather(grad_cols, "tp", axis=1, tiled=True)
    active_gate, pullback = jax.vjp(jax.nn.gelu, gate_branch.astype(jnp.float32))
    mixed_in = (active_gate * states).astype(jnp.bfloat16)
    piece_cols = grad_tokens
    grad_out_proj = lax.psum_scatter(
        contract_rows(piece_cols, mixed_in).astype(jnp.bfloat16),
        "sp",
        scatter_dimension=0,
        tiled=True,
    ).astype(jnp.float32)
    piece_cols = grad_tokens
    grad_mixed = jnp.dot(
        piece_cols,
        lax.all_gather(out_proj, "sp", axis=0, tiled=True),
        preferred_element_type=jnp.float32,
    )
    grad_gate_branch = pullback(grad_mixed * states)[0].astype(jnp.bfloat16)
    grad_state = grad_mixed * active_gate
    decays = jnp.exp(log_decay)
    next_decay = jnp.concatenate([decays[1:], jnp.ones_like(decays[:1])], axis=0)
    span_flip, local_flip = lax.associative_scan(
        combine_pair, (jnp.flip(next_decay, 0), jnp.flip(grad_state, 0))
    )
    span_decay = jnp.flip(span_flip, 0)
    local_grad = jnp.flip(local_flip, 0)
    whole_decay = span_decay[0] * decays[0]
    entry_term = decays[0] * local_grad[0]
    carried = carried_in(
        (whole_decay, entry_term),
        "sp",
        compose_maps,
        (jnp.ones_like(whole_decay), jnp.zeros_like(entry_term)),
    )
    grad_input_term = local_grad + span_decay * carried[1][None, :]
    earlier_state = from_behind(states[-1:], "sp", 1)
    prev_states = jnp.concatenate([earlier_state, states[:-1]], axis=0)
    grad_log_decay = (grad_input_term * decays * prev_states).astype(jnp.bfloat16)
    return (
        grad_gate_w[None],
        grad_up_w[None],
        grad_down[None],
        grad_out_proj,
        grad_gate_branch,
        grad_log_decay,
        grad_input_term,
    )


def solution(mesh):
    return jax.shard_map(
        shards,
        mesh=mesh,
        in_specs=(
            P("sp", "tp"),
            P("sp", "tp"),
            P("sp", None),
            P("sp", None),
            P("sp", "tp"),
            P("sp", "tp"),
            P("sp", "tp"),
            P("sp", None, "tp"),
            P("sp", None, "tp"),
            P("sp", "tp", None),
            P("sp", "tp"),
        ),
        out_specs=(
            P("sp", None, "tp"),
            P("sp", None, "tp"),
            P("sp", "tp", None),
            P("sp", "tp"),
            P("sp", "tp"),
            P("sp", "tp"),
            P("sp", "tp"),
        ),
        check_vma=False,
    )
```

profile of v0, /device:TPU:0, one launch (start us, length us, event | category | flops | bytes accessed | tf_op | source)
XLA Modules:
  0.0 252.5 jit_solution(4397792106868432355)
XLA Ops:
  16.4 17.4 %all_to_all.15 = bf16[8,40,512]{2,1,0:T(8,128)(2,1)} all-to-all(bf16[8,40,512]{2,1,0:T(8,128)(2,1)S(1)} %broadcast_select_fusion), channel_id=1, replica_groups=mesh['sp'=8,'tp'=4] {'sp'}, dimensions={0} | all-to-all | bytes 655360 | tf_op jit(solution)/shard_map/all_to_all | solution.py:86
  37.8 14.2 %all_to_all.16 = bf16[8,40,512]{2,1,0:T(8,128)(2,1)} all-to-all(bf16[8,40,512]{2,1,0:T(8,128)(2,1)S(1)} %fusion.12), channel_id=1, replica_groups=mesh['sp'=8,'tp'=4] {'sp'}, dimensions={0} | all-to-all | bytes 655360 | tf_op jit(solution)/shard_map/all_to_all | solution.py:93
  52.0 9.4 %all-gather.6.cloned.1.call-done = bf16[8,40,2048]{2,1,0:T(8,128)(2,1)} async-done(((bf16[8,40,512]{2,1,0:T(8,128)(2,1)}), bf16[8,40,2048]{2,1,0:T(8,128)(2,1)}) %all-gather.6.cloned.1.call-update) | async-done | bytes 1310736 | tf_op jit(solution)/shard_map/all_gather | solution.py:98
  61.4 3.8 %fusion.51 = f32[320,512]{1,0:T(8,128)} fusion(bf16[320,2048]{1,0:T(8,128)(2,1)} %bitcast.60, bf16[1,2048,512]{2,1,0:T(8,128)(2,1)} %param.20), kind=kOutput, calls=%fused_computation.129 | convolution fusion | flops 671088640 | bytes 4063232 | tf_op jit(solution)/shard_map/dot_general | solution.py:106
  66.9 24.9 %all-gather.8.cloned.1.call-done = bf16[8,40,2048]{2,1,0:T(8,128)(2,1)} async-done(((bf16[8,40,512]{2,1,0:T(8,128)(2,1)}), bf16[8,40,2048]{2,1,0:T(8,128)(2,1)}) %all-gather.8.cloned.1.call-update) | async-done | bytes 1310736 | tf_op jit(solution)/shard_map/all_gather | solution.py:99
  91.8 2.9 %multiply_convert_fusion.1 = (bf16[320,512]{1,0:T(8,128)(2,1)S(1)}, bf16[320,512]{1,0:T(8,128)(2,1)S(1)}) fusion(f32[320,512]{1,0:T(8,128)} %fusion.51, f32[320,512]{1,0:T(8,128)} %fusion.53, bf16[320,2048]{1,0:T(8,128)(2,1)} %bitcast.77, bf16[1,512,2048]{2,1,0:T(8,128)(2,1)S(1)} %copy-done), kind=kOutput, calls=%fused_computation.31 | convolution fusion | flops 673218560 | bytes 5373952 | tf_op jit(solution)/shard_map/dot_general | solution.py:49
  94.8 2.6 %fusion.4 = bf16[320,2048]{1,0:T(8,128)(2,1)} fusion(bf16[2048,512]{1,0:T(8,128)(2,1)S(1)} %bitcast.76, bf16[2048,512]{1,0:T(8,128)(2,1)S(1)} %bitcast.75, bf16[320,512]{1,0:T(8,128)(2,1)S(1)} %get-tuple-element.134, bf16[320,512]{1,0:T(8,128)(2,1)S(1)} %get-tuple-element.135), kind=kOutput, calls=%fused_computation.17 | convolution fusion | flops 1352531968 | bytes 6160384 | tf_op jit(solution)/shard_map/dot_general | solution.py:49
  109.0 2.9 %slice.259 = f32[64,640]{1,0:T(8,128)} reverse(f32[64,640]{1,0:T(8,128)} %slice.258), dimensions={0} | reverse | bytes 327680 | tf_op jit(solution)/shard_map/slice | solution.py:151
  112.0 3.0 %slice.250 = f32[63,640]{1,0:T(8,128)} reverse(f32[63,640]{1,0:T(8,128)} %slice.249), dimensions={0} | reverse | bytes 322560 | tf_op jit(solution)/shard_map/slice | solution.py:151
  114.9 2.9 %slice.252 = f32[64,640]{1,0:T(8,128)} reverse(f32[64,640]{1,0:T(8,128)} %slice.251), dimensions={0} | reverse | bytes 327680 | tf_op jit(solution)/shard_map/slice | solution.py:151
  117.9 4.3 %convolution_bitcast_fusion.2 = f32[1,2048,512]{2,1,0:T(8,128)} fusion(bf16[320,2048]{1,0:T(8,128)(2,1)S(1)} %bitcast.63, bf16[320,512]{1,0:T(8,128)(2,1)} %copy-done.11), kind=kOutput, calls=%fused_computation.15 | convolution fusion | flops 671088640 | bytes 5832704 | tf_op jit(solution)/shard_map/dot_general | solution.py:43
  122.2 4.9 %reduce-scatter.3.cloned.1.call-done = bf16[8,40,512]{2,1,0:T(8,128)(2,1)} async-done(((bf16[8,40,2048]{2,1,0:T(8,128)(2,1)}), bf16[8,40,512]{2,1,0:T(8,128)(2,1)}) %reduce-scatter.3.cloned.1.call-update) | async-done | bytes 327696 | tf_op jit(solution)/shard_map/reduce_scatter | solution.py:119
  127.1 4.6 %all-to-all-start.2 = ((bf16[8,40,512]{2,1,0:T(8,128)(2,1)}), bf16[8,40,512]{2,1,0:T(8,128)(2,1)S(1)}, u32[]{:S(2)}, u32[]{:S(2)}) async-start(bf16[8,40,512]{2,1,0:T(8,128)(2,1)} %reduce-scatter.3.cloned.1.call-done), calls=%async_computation.3 | async-start | bytes 655360 | tf_op jit(solution)/shard_map/all_to_all | solution.py:125
  132.0 4.8 %convolution_bitcast_fusion.1 = f32[1,2048,512]{2,1,0:T(8,128)} fusion(bf16[320,2048]{1,0:T(8,128)(2,1)} %bitcast.61, bf16[320,512]{1,0:T(8,128)(2,1)} %copy-done.10), kind=kOutput, calls=%fused_computation.14 | convolution fusion | flops 671088640 | bytes 5832704 | tf_op jit(solution)/shard_map/dot_general | solution.py:43
  136.8 3.4 %convolution_bitcast_fusion = f32[1,512,2048]{2,1,0:T(8,128)} fusion(bf16[320,2048]{1,0:T(8,128)(2,1)S(1)} %bitcast.78, f32[320,512]{1,0:T(8,128)S(1)} %copy-done.24, f32[320,512]{1,0:T(8,128)S(1)} %copy-done.23), kind=kOutput, calls=%fused_computation.13 | convolution fusion | flops 672071680 | bytes 6815744 | tf_op jit(solution)/shard_map/dot_general | solution.py:43
  140.2 2.7 %all-to-all-done.2 = bf16[8,40,512]{2,1,0:T(8,128)(2,1)S(1)} async-done(((bf16[8,40,512]{2,1,0:T(8,128)(2,1)}), bf16[8,40,512]{2,1,0:T(8,128)(2,1)S(1)}, u32[]{:S(2)}, u32[]{:S(2)}) %all-to-all-start.2) | async-done | bytes 327712 | tf_op jit(solution)/shard_map/all_to_all | solution.py:125
  145.0 10.4 %all_gather.22 = bf16[128,2048]{1,0:T(8,128)(2,1)S(1)} all-gather(bf16[128,512]{1,0:T(8,128)(2,1)S(1)} %add_convert_fusion), channel_id=1, replica_groups=mesh['sp'=8,'tp'=4] {'tp'}, dimensions={1}, use_global_device_ids=true | all-gather | bytes 655360 | tf_op jit(solution)/shard_map/all_gather | solution.py:131
  155.3 3.1 %fusion.24 = (f32[128,640]{1,0:T(8,128)S(1)}, bf16[128,640]{1,0:T(8,128)(2,1)}) fusion(bf16[128,640]{1,0:T(8,128)(2,1)} %param.17, f32[128,640]{1,0:T(8,128)S(1)} %copy-done.4, bf16[128,2048]{1,0:T(8,128)(2,1)S(1)} %all_gather.22, bf16[2048,640]{1,0:T(8,128)(2,1)} %all-gather.10.cloned.1.call-done), kind=kOutput, calls=%fused_computation.50 | convolution fusion | flops 337510400 | bytes 4128768 | tf_op jit(solution)/shard_map/dot_general | solution.py:142
  159.9 2.9 %slice.254 = f32[64,640]{1,0:T(8,128)} reverse(f32[64,640]{1,0:T(8,128)} %slice.253), dimensions={0} | reverse | bytes 327680 | tf_op jit(solution)/shard_map/slice | solution.py:151
  162.9 2.9 %slice.256 = f32[64,640]{1,0:T(8,128)} reverse(f32[64,640]{1,0:T(8,128)} %slice.255), dimensions={0} | reverse | bytes 327680 | tf_op jit(solution)/shard_map/slice | solution.py:151
  183.2 3.3 %convolution_convert_fusion = bf16[2048,640]{1,0:T(8,128)(2,1)} fusion(bf16[128,2048]{1,0:T(8,128)(2,1)S(1)} %all_gather.22, f32[128,640]{1,0:T(8,128)S(1)} %copy-done.4, bf16[128,640]{1,0:T(8,128)(2,1)} %param.17), kind=kOutput, calls=%fused_computation.16 | convolution fusion | flops 337756160 | bytes 3637248 | tf_op jit(solution)/shard_map/dot_general | solution.py:43
  205.8 14.0 %all-gather.1 = f32[8,1,640]{2,1,0:T(1,128)S(1)} all-gather(f32[1,1,640]{2,1,0:T(1,128)S(1)} %get-tuple-element.138), channel_id=1, replica_groups=mesh['sp'=8,'tp'=4] {'sp'}, dimensions={0}, use_global_device_ids=true | all-gather | bytes 23040 | tf_op jit(solution)/shard_map/all_gather | solution.py:9
  219.8 13.9 %all-gather = f32[8,1,640]{2,1,0:T(1,128)S(1)} all-gather(f32[1,1,640]{2,1,0:T(1,128)S(1)} %get-tuple-element.139), channel_id=1, replica_groups=mesh['sp'=8,'tp'=4] {'sp'}, dimensions={0}, use_global_device_ids=true | all-gather | bytes 23040 | tf_op jit(solution)/shard_map/all_gather | solution.py:9
  236.9 2.5 %rev.16 = f32[128,640]{1,0:T(8,128)S(1)} reverse(f32[128,640]{1,0:T(8,128)} %add.255), dimensions={0} | reverse | bytes 655360 | tf_op jit(solution)/shard_map/jit(_flip)/rev | solution.py:154
  (231 shorter events, 75.1 us)
Async XLA Ops:
  8.0 83.8 %copy-start = (bf16[1,512,2048]{2,1,0:T(8,128)(2,1)S(1)}, bf16[1,512,2048]{2,1,0:T(8,128)(2,1)}, u32[]{:S(2)}) copy-start(bf16[1,512,2048]{2,1,0:T(8,128)(2,1)} %param.22) | copy-start | bytes 6291460
  8.0 6.2 %copy-start.2 = (bf16[128,512]{1,0:T(8,128)(2,1)S(1)}, bf16[128,512]{1,0:T(8,128)(2,1)}, u32[]{:S(2)}) copy-start(bf16[128,512]{1,0:T(8,128)(2,1)} %param.13) | copy-start | bytes 393220
  8.0 53.4 %all-gather.6.cloned.1.call-start = ((), (), s32[]{:S(2)}) async-start(), calls=%async_computation.5 | async-start | bytes 1638400 | tf_op jit(solution)/shard_map/all_gather | solution.py:98
  14.2 19.6 %copy-start.18 = (f32[128,2]{0,1:T(2,128)S(1)}, f32[128,2]{0,1:T(2,128)}, u32[]{:S(2)}) copy-start(f32[128,2]{0,1:T(2,128)} %param.16) | copy-start | bytes 3076
  14.2 21.4 %copy-start.1 = (bf16[128,512]{1,0:T(8,128)(2,1)S(1)}, bf16[128,512]{1,0:T(8,128)(2,1)}, u32[]{:S(2)}) copy-start(bf16[128,512]{1,0:T(8,128)(2,1)} %param.14) | copy-start | bytes 393220
  33.8 58.0 %all-gather.8.cloned.1.call-start = ((), (), s32[]{:S(2)}) async-start(), calls=%async_computation.6 | async-start | bytes 1638400 | tf_op jit(solution)/shard_map/all_gather | solution.py:99
  52.0 75.1 %reduce-scatter.3.cloned.1.call-start = ((), (), s32[]{:S(2)}) async-start(), calls=%async_computation.7 | async-start | bytes 1638400 | tf_op jit(solution)/shard_map/reduce_scatter | solution.py:119
  61.4 3.8 %copy-start.3 = (bf16[8,40,2048]{2,1,0:T(8,128)(2,1)S(1)}, bf16[8,40,2048]{2,1,0:T(8,128)(2,1)}, u32[]{:S(2)}) copy-start(bf16[8,40,2048]{2,1,0:T(8,128)(2,1)} %all-gather.6.cloned.1.call-done) | copy-start | bytes 3932164
  61.4 3.8 %copy-start.20 = (bf16[1,2048,512]{2,1,0:T(8,128)(2,1)S(1)}, bf16[1,2048,512]{2,1,0:T(8,128)(2,1)}, u32[]{:S(2)}) copy-start(bf16[1,2048,512]{2,1,0:T(8,128)(2,1)} %param.21) | copy-start | bytes 6291460
  91.8 2.9 %copy-start.19 = (bf16[1,2048,512]{2,1,0:T(8,128)(2,1)S(1)}, bf16[1,2048,512]{2,1,0:T(8,128)(2,1)}, u32[]{:S(2)}) copy-start(bf16[1,2048,512]{2,1,0:T(8,128)(2,1)} %param.20) | copy-start | bytes 6291460
  91.8 3.0 %copy-start.21 = (bf16[1,2048,512]{2,1,0:T(8,128)(2,1)S(1)}, bf16[1,2048,512]{2,1,0:T(8,128)(2,1)}, u32[]{:S(2)}) copy-start(bf16[1,2048,512]{2,1,0:T(8,128)(2,1)} %param.21) | copy-start | bytes 6291460
  97.5 57.9 %all-gather.10.cloned.1.call-start = ((), (), s32[]{:S(2)}) async-start(), calls=%async_computation.9 | async-start | bytes 2949120 | tf_op jit(solution)/shard_map/all_gather | solution.py:144
  99.4 142.6 %collective-permute-start = (f32[1,640]{1,0:T(1,128)}, f32[1,640]{1,0:T(1,128)}, u32[]{:S(2)}, u32[]{:S(2)}) collective-permute-start(f32[1,640]{1,0:T(1,128)} %slice.320), channel_id=1, source_target_pairs={{0,4},{4,8},{8,12},{12,16},{16,20},{20,24},{24,28},{1,5},{5,9},{9,... | collective-permute-start | bytes 7688 | tf_op jit(solution)/shard_map/ppermute | solution.py:26
  127.1 15.7 %all-to-all-start.2 = ((bf16[8,40,512]{2,1,0:T(8,128)(2,1)}), bf16[8,40,512]{2,1,0:T(8,128)(2,1)S(1)}, u32[]{:S(2)}, u32[]{:S(2)}) async-start(bf16[8,40,512]{2,1,0:T(8,128)(2,1)} %reduce-scatter.3.cloned.1.call-done), calls=%async_computation.3 | async-start | bytes 655360 | tf_op jit(solution)/shard_map/all_to_all | solution.py:125
  131.7 5.1 %copy-start.23 = (f32[320,512]{1,0:T(8,128)S(1)}, f32[320,512]{1,0:T(8,128)}, u32[]{:S(2)}) copy-start(f32[320,512]{1,0:T(8,128)} %fusion.51) | copy-start | bytes 1966084
  131.7 111.8 %reduce-scatter.5.cloned.1.call-start = ((), (), s32[]{:S(2)}) async-start(), calls=%async_computation.8 | async-start | bytes 2949120 | tf_op jit(solution)/shard_map/reduce_scatter | solution.py:135
  131.9 4.8 %copy-start.22 = (bf16[8,40,2048]{2,1,0:T(8,128)(2,1)S(1)}, bf16[8,40,2048]{2,1,0:T(8,128)(2,1)}, u32[]{:S(2)}) copy-start(bf16[8,40,2048]{2,1,0:T(8,128)(2,1)} %all-gather.8.cloned.1.call-done) | copy-start | bytes 3932164
  132.0 4.8 %copy-start.24 = (f32[320,512]{1,0:T(8,128)S(1)}, f32[320,512]{1,0:T(8,128)}, u32[]{:S(2)}) copy-start(f32[320,512]{1,0:T(8,128)} %fusion.53) | copy-start | bytes 1966084
  142.8 12.5 %copy-start.4 = (f32[128,640]{1,0:T(8,128)S(1)}, f32[128,640]{1,0:T(8,128)}, u32[]{:S(2)}) copy-start(f32[128,640]{1,0:T(8,128)} %param.19) | copy-start | bytes 983044
  158.4 4.4 %copy-start.7 = (f32[128,640]{1,0:T(8,128)}, f32[128,640]{1,0:T(8,128)S(1)}, u32[]{:S(2)}) copy-start(f32[128,640]{1,0:T(8,128)S(1)} %get-tuple-element.136) | copy-start | bytes 983044
  189.9 7.5 %copy-start.12 = (f32[31,640]{1,0:T(8,128)S(1)}, f32[31,640]{1,0:T(8,128)}, u32[]{:S(2)}) copy-start(f32[31,640]{1,0:T(8,128)} %slice.301) | copy-start | bytes 238084
  194.6 3.5 %copy-start.17 = (f32[1,640]{1,0:T(1,128)S(1)}, f32[1,640]{1,0:T(1,128)}, u32[]{:S(2)}) copy-start(f32[1,640]{1,0:T(1,128)} %slice.353) | copy-start | bytes 7684
  196.0 5.5 %copy-start.9 = (f32[63,640]{1,0:T(8,128)S(1)}, f32[63,640]{1,0:T(8,128)}, u32[]{:S(2)}) copy-start(f32[63,640]{1,0:T(8,128)} %slice.250) | copy-start | bytes 483844
  236.1 5.9 %copy-start.6 = (f32[128,640]{1,0:T(8,128)S(1)}, f32[128,640]{1,0:T(8,128)}, u32[]{:S(2)}) copy-start(f32[128,640]{1,0:T(8,128)} %param.18) | copy-start | bytes 983044
  (8 other events, 10.4 us)
Sparse Core Ops, SparseCore 0:
  33.9 27.4 all-gather.5
  63.3 28.5 all-gather.7
  97.6 29.4 reduce-scatter.2
Sparse Core Ops, SparseCore 1:
  99.6 33.5 all-gather.9
  186.6 35.5 reduce-scatter.4
where the time goes:
time: 256 us; the launch traced here: 252 us
  blocking collectives  69.8 us (27%)
  local copies, waits for them, and re-layouts  68.4 us (27%)
  waiting for transfers between devices  42.5 us (17%)
  matrix products  29.8 us (12%)
  other arithmetic  18.7 us (7%)
  between operations  15.9 us (6%)
  starting transfers between devices  7.14 us (3%)
    slice x49, local copies, waits for them, and re-layouts, shards(): lax.associative_scan(combine_pair, (jnp.flip(next_decay, 0), jnp.flip(gra...  40.8 us
    all_gather x2, blocking collectives, carried_in(): pieces = jax.tree.map(lambda part: lax.all_gather(part, axis), value)  27.9 us
    all_gather x1, waiting for transfers between devices, shards(): lax.all_gather(part_cot, 'tp', axis=2, tiled=True)  24.9 us
    all_to_all x1, blocking collectives, shards(): lax.all_to_all(send_data.reshape(groups, room, col_width), 'sp', split_ax...  17.4 us
    dot_general x4, matrix products, contract_rows(): lax.dot_general(left_mat, right_mat, (((0,), (0,)), ((), ())), preferred_...  15.8 us
    all_to_all x1, blocking collectives, shards(): lax.all_to_all(send_cot.reshape(groups, room, col_width), 'sp', split_axi...  14.2 us
    all_gather x1, blocking collectives, shards(): grad_tokens = lax.all_gather(grad_cols, 'tp', axis=1, tiled=True)  10.4 us
    all_gather x1, waiting for transfers between devices, shards(): lax.all_gather(part_rows, 'tp', axis=2, tiled=True)  9.4 us
  transfers between devices with their start and end apart: 7, of which 4 were waited for; matrix products, arithmetic and copies ran while one was open for 40% of the time, Pallas kernels for 0%

commit v1 on v0

v1 whole, which is shorter than its diff:
```python
import jax
import jax.numpy as jnp
from jax import lax
from jax.experimental import pallas as pl
from jax.experimental.pallas import tpu as pltpu
from jax.sharding import PartitionSpec as P

BF = jnp.bfloat16
F32 = jnp.float32
CORES = 2
GELU_C = 0.7978845608028654
GELU_A = 0.044715


def silu_parts(pre_gate):
    sigmoid_val = jax.nn.sigmoid(pre_gate)
    return (pre_gate * sigmoid_val, sigmoid_val * (1.0 + pre_gate * (1.0 - sigmoid_val)))


def contract_rows(left_mat, right_mat):
    return lax.dot_general(
        left_mat, right_mat, (((0,), (0,)), ((), ())), preferred_element_type=F32
    )


def contract_cols(left_mat, right_mat):
    return lax.dot_general(
        left_mat, right_mat, (((1,), (1,)), ((), ())), preferred_element_type=F32
    )


def gelu_parts(x):
    t = jnp.tanh(GELU_C * (x + GELU_A * (x * x * x)))
    half = 0.5 * (1.0 + t)
    slope = half + 0.5 * x * (1.0 - t * t) * (GELU_C * (1.0 + 3.0 * GELU_A * x * x))
    return x * half, slope


def selection(routes_t, weights_t, groups, room):
    picks, toks = routes_t.shape
    experts = lax.broadcasted_iota(jnp.int32, (groups, toks), 0)
    named = jnp.zeros((groups, toks), F32)
    weight = jnp.zeros((groups, toks), F32)
    for k in range(picks):
        hit = routes_t[k : k + 1, :] == experts
        named = named + jnp.where(hit, 1.0, 0.0)
        weight = weight + jnp.where(hit, weights_t[k : k + 1, :], 0.0)
    rows = lax.broadcasted_iota(jnp.int32, (toks, toks), 0)
    cols = lax.broadcasted_iota(jnp.int32, (toks, toks), 1)
    before = jnp.where(rows < cols, 1.0, 0.0).astype(BF)
    slot = jnp.dot(named.astype(BF), before, preferred_element_type=F32)
    slot = jnp.where(named > 0.5, slot, -1.0)
    place = lax.broadcasted_iota(jnp.int32, (room, toks), 0).astype(F32)
    picked, column = [], []
    for e in range(groups):
        one = jnp.where(slot[e : e + 1, :] == place, 1.0, 0.0)
        picked.append(one)
        column.append(jnp.sum(one * weight[e : e + 1, :], axis=1, keepdims=True))
    return jnp.concatenate(picked, axis=0).astype(BF), jnp.concatenate(column, axis=0)


def greet(groups, parts, mine, col):
    barrier = pltpu.get_barrier_semaphore()
    for d in range(1, groups):
        pl.semaphore_signal(
            barrier, inc=1, device_id={"sp": lax.rem(mine + d, groups)},
            device_id_type=pl.DeviceIdType.MESH,
        )
    for d in range(1, parts):
        pl.semaphore_signal(
            barrier, inc=1, device_id={"tp": lax.rem(col + d, parts)},
            device_id_type=pl.DeviceIdType.MESH,
        )
    pl.semaphore_wait(barrier, groups + parts - 2)


def remote(src, dst, send, recv, axis, peer):
    return pltpu.make_async_remote_copy(
        src_ref=src, dst_ref=dst, send_sem=send, recv_sem=recv,
        device_id={axis: peer}, device_id_type=pl.DeviceIdType.MESH,
    )


def dispatch_kernel(
    groups, parts, room,
    x_ref, cot_ref, routes_ref, weights_ref, gate_ref, states_ref, proj_ref,
    rows_ref, scaled_ref, proj_all, mixed_all,
    out_x, out_c, in_x, in_c, mix_own,
    a_send, a_recv, t_send, t_recv, z_send, z_recv, c_send, c_recv, l_sem,
):
    mine, col = lax.axis_index("sp"), lax.axis_index("tp")
    width = x_ref.shape[1]
    depth = groups // CORES
    z, core = mine // CORES, lax.rem(mine, CORES)
    picked, weight = selection(routes_ref[...], weights_ref[...], groups, room)
    got = jnp.dot(picked, x_ref[...], preferred_element_type=F32).astype(BF)
    got_c = jnp.dot(picked, cot_ref[...], preferred_element_type=F32)
    got_c = (got_c * weight).astype(BF)
    for e in range(groups):
        out_x[e] = got[e * room : (e + 1) * room]
        out_c[e] = got_c[e * room : (e + 1) * room]
    act, _ = gelu_parts(gate_ref[...].astype(F32))
    mix_own[...] = (act * states_ref[...]).astype(BF)
    greet(groups, parts, mine, col)

    waits = []
    own = []
    for a, (src, dst) in enumerate(((out_x, in_x), (out_c, in_c))):
        for d in range(1, groups):
            peer = lax.rem(mine + d, groups)
            c = remote(src.at[peer], dst.at[mine], a_send.at[a, d], a_recv.at[a, d], "sp", peer)
            c.start()
            waits.append(c)
        o = pltpu.make_async_copy(src.at[mine], dst.at[mine], l_sem.at[a])
        o.start()
        own.append(o)
    for a, (src, dst) in enumerate(((mix_own, mixed_all), (proj_ref, proj_all))):
        o = pltpu.make_async_copy(src, dst.at[mine], l_sem.at[2 + a])
        o.start()
        own.append(o)
    own[2].wait()
    own[3].wait()

    pairs = (mixed_all, proj_all)

    def chain(step, wait):
        for a, buf in enumerate(pairs):
            right = buf.at[jnp.maximum(z - step, 0) * CORES + core]
            left = buf.at[jnp.minimum(z + step, depth - 1) * CORES + core]
            go_r = jnp.logical_and(z - step >= 0, z + 1 < depth)
            go_l = jnp.logical_and(z + step < depth, z >= 1)
            up = jnp.minimum(z + 1, depth - 1) * CORES + core
            down = jnp.maximum(z - 1, 0) * CORES + core

            def c_r():
                return remote(right, right, z_send.at[a, 0, step], z_recv.at[a, 0, step], "sp", up)

            def c_l():
                return remote(left, left, z_send.at[a, 1, step], z_recv.at[a, 1, step], "sp", down)

            @pl.when(go_r)
            def _():
                c_r().wait_send() if wait else c_r().start()

            @pl.when(go_l)
            def _():
                c_l().wait_send() if wait else c_l().start()

    def arrived(step):
        for a, buf in enumerate(pairs):
            from_l = buf.at[jnp.maximum(z - 1 - step, 0) * CORES + core]
            from_r = buf.at[jnp.minimum(z + 1 + step, depth - 1) * CORES + core]
            for way, ok, ref in (
                (0, z - 1 - step >= 0, from_l),
                (1, z + 1 + step < depth, from_r),
            ):
                @pl.when(ok)
                def _(way=way, ref=ref, a=a):
                    remote(ref, ref, z_send.at[a, way, step], z_recv.at[a, way, step],
                           "sp", lax.rem(mine + 1, groups)).wait_recv()

    partner = z * CORES + (1 - core)

    def across(step, way, mode):
        for a, buf in enumerate(pairs):
            ok = z - step >= 0 if way == 0 else z + step < depth
            zz = jnp.maximum(z - step, 0) if way == 0 else jnp.minimum(z + step, depth - 1)
            ref = buf.at[zz * CORES + (1 - core if mode == "recv" else core)]

            @pl.when(ok)
            def _():
                c = remote(ref, ref, c_send.at[a, way, step], c_recv.at[a, way, step], "sp", partner)
                if mode == "start":
                    c.start()
                elif mode == "send":
                    c.wait_send()
                else:
                    c.wait_recv()

    chain(0, False)
    across(0, 0, "start")

    tp_waits = []
    here = pl.ds(pl.multiple_of(col * width, width), width)
    for a, (src, dst) in enumerate(((in_x, rows_ref), (in_c, scaled_ref))):
        own[a].wait()
        for c in waits[a * (groups - 1) : (a + 1) * (groups - 1)]:
            c.wait_recv()
        for d in range(1, parts):
            c = remote(src, dst.at[:, :, here], t_send.at[a, d], t_recv.at[a, d], "tp",
                       lax.rem(col + d, parts))
            c.start()
            tp_waits.append(c)
        o = pltpu.make_async_copy(src, dst.at[:, :, here], l_sem.at[4 + a])
        o.start()
        own.append(o)
    for step in range(depth - 1):
        arrived(step)
        if step + 1 < depth - 1:
            chain(step + 1, False)
        across(step + 1, 0, "start")
        across(step + 1, 1, "start")
    for c in waits:
        c.wait_send()
    for c in tp_waits:
        c.wait()
    own[4].wait()
    own[5].wait()
    for step in range(depth - 1):
        chain(step, True)
    for step in range(depth):
        for way in range(2):
            if step == 0 and way == 1:
                continue
            across(step, way, "send")
            across(step, way, "recv")


def finish_kernel(
    groups, parts, room,
    terms_ref, cot_ref, routes_ref, weights_ref, gate_ref, states_ref, decay_ref, proj_ref, mixed_ref,
    outp_ref, ggate_ref, gdecay_ref, gin_ref,
    shares, summed, back, flipped, blocks, carry_own, carry_in, prev_in,
    s_send, s_recv, a_send, a_recv, g_send, g_recv, b_send, b_recv, k_send, k_recv, p_send, p_recv, l_sem,
):
    mine, col = lax.axis_index("sp"), lax.axis_index("tp")
    toks, width = cot_ref.shape
    greet(groups, parts, mine, col)

    def near(width_of, index):
        return pl.ds(pl.multiple_of(index * width_of, width_of), width_of)

    nxt = lax.rem(mine + 1, groups)
    prev_copy = remote(states_ref.at[pl.ds(toks - 8, 8)], prev_in, p_send, p_recv, "sp", nxt)
    share_copies = []
    for d in range(1, parts):
        peer = lax.rem(col + d, parts)
        c = remote(terms_ref.at[:, :, near(width, peer)], shares.at[d - 1], s_send.at[d], s_recv.at[d],
                   "tp", peer)
        c.start()
        share_copies.append(c)
    prev_copy.start()
    picked, _ = selection(routes_ref[...], weights_ref[...], groups, room)
    rows = lax.broadcasted_iota(jnp.int32, (toks, toks), 0)
    cols = lax.broadcasted_iota(jnp.int32, (toks, toks), 1)
    eye = jnp.where(rows == cols, 1.0, 0.0).astype(BF)
    act, slope = gelu_parts(gate_ref[...].astype(F32))
    decays = jnp.exp(decay_ref[...])
    for c in share_copies:
        c.wait_recv()
    for g in range(groups):
        total = terms_ref[g, :, near(width, col)].astype(F32)
        for d in range(1, parts):
            total = total + shares[d - 1, g].astype(F32)
        summed[g] = total.astype(BF)
    back_copies = []
    for d in range(1, groups):
        peer = lax.rem(mine + d, groups)
        c = remote(summed.at[peer], back.at[mine], a_send.at[d], a_recv.at[d], "sp", peer)
        c.start()
        back_copies.append(c)
    o = pltpu.make_async_copy(summed.at[mine], back.at[mine], l_sem.at[0])
    o.start()
    o.wait()
    for c in back_copies:
        c.wait_recv()
    total = contract_rows(cot_ref[...], eye)
    for g in range(groups):
        total = total + contract_rows(back[g], picked[g * room : (g + 1) * room])
    flipped[near(width, col), :] = total.astype(BF)
    grad_copies = []
    for d in range(1, parts):
        part = flipped.at[near(width, col)]
        c = remote(part, part, g_send.at[d], g_recv.at[d], "tp", lax.rem(col + d, parts))
        c.start()
        grad_copies.append(c)
    for c in grad_copies:
        c.wait_recv()
    high = flipped.shape[0] // groups
    block_copies = []
    for d in range(1, groups):
        peer = lax.rem(mine + d, groups)
        c = remote(flipped.at[near(high, peer)], blocks.at[mine], b_send.at[d], b_recv.at[d], "sp", peer)
        c.start()
        block_copies.append(c)
    o = pltpu.make_async_copy(flipped.at[near(high, mine)], blocks.at[mine], l_sem.at[1])
    o.start()
    grad_mixed = contract_rows(flipped[...], proj_ref[...])
    states = states_ref[...]
    ggate_ref[...] = (grad_mixed * states * slope).astype(BF)
    local = grad_mixed * act
    line = lax.broadcasted_iota(jnp.int32, local.shape, 0)
    span = jnp.where(line < toks - 1, pltpu.roll(decays, toks - 1, 0), 1.0)
    k = 1
    while k < toks:
        inside = line < toks - k
        local = local + span * jnp.where(inside, pltpu.roll(local, toks - k, 0), 0.0)
        span = span * jnp.where(inside, pltpu.roll(span, toks - k, 0), 1.0)
        k *= 2
    eight = lax.broadcasted_iota(jnp.int32, (8, local.shape[1]), 0)
    whole = span[0:1] * decays[0:1]
    entry = local[0:1] * decays[0:1]
    carry_own[...] = jnp.where(eight == 0, whole, entry)
    carry_copies = []
    for d in range(1, groups):
        peer = lax.rem(mine + d, groups)
        c = remote(carry_own, carry_in.at[d - 1], k_send.at[d], k_recv.at[d], "sp", peer)
        c.start()
        carry_copies.append(c)
    prev_copy.wait_recv()
    first = jnp.where(mine > 0, prev_in[7:8, :], 0.0)
    prev = jnp.where(line == 0, first, pltpu.roll(states, 1, 0))
    for c in carry_copies:
        c.wait_recv()
    carried = jnp.zeros_like(whole)
    for ahead in range(groups - 1, 0, -1):
        got = carry_in[groups - ahead - 1]
        carried = jnp.where(mine + ahead < groups, got[1:2] + got[0:1] * carried, carried)
    grad_in = local + span * carried
    gin_ref[...] = grad_in
    gdecay_ref[...] = (grad_in * decays * prev).astype(BF)
    o.wait()
    for c in block_copies:
        c.wait_recv()
    total = jnp.dot(blocks[0], mixed_ref[0], preferred_element_type=F32)
    for g in range(1, groups):
        total = total + jnp.dot(blocks[g], mixed_ref[g], preferred_element_type=F32)
    outp_ref[...] = total
    for c in [prev_copy] + share_copies + back_copies + grad_copies + block_copies + carry_copies:
        c.wait_send()


def shards(
    moe_input, cotangent, routes, route_weights, gate_branch, log_decay, states,
    w_gate, w_up, w_down, out_proj,
):
    groups, parts = lax.axis_size("sp"), lax.axis_size("tp")
    tok_rows, picks = routes.shape
    width = moe_input.shape[1]
    model = width * parts
    chans = states.shape[1]
    room = tok_rows * picks * 5 // (4 * groups)
    room = (room + 7) // 8 * 8
    depth = groups // CORES
    high = out_proj.shape[0]
    routes_t, weights_t = routes.T, route_weights.T
    vmem = pl.BlockSpec(memory_space=pltpu.VMEM)
    dma = pltpu.SemaphoreType.DMA

    def kernel_of(body, name):
        def run(*refs):
            body(groups, parts, room, *refs)
        run.__name__ = name
        return run

    rows_in, cot_in, proj_all, mixed_all = pl.pallas_call(
        kernel_of(dispatch_kernel, "dispatch"),
        out_shape=[
            jax.ShapeDtypeStruct((groups, room, model), BF),
            jax.ShapeDtypeStruct((groups, room, model), BF),
            jax.ShapeDtypeStruct((groups, high, chans), BF),
            jax.ShapeDtypeStruct((groups, tok_rows, chans), BF),
        ],
        in_specs=[vmem] * 7,
        out_specs=[vmem] * 4,
        scratch_shapes=[pltpu.VMEM((groups, room, width), BF)] * 4
        + [pltpu.VMEM((tok_rows, chans), BF)]
        + [dma((2, groups))] * 2 + [dma((2, parts))] * 2
        + [dma((2, 2, depth))] * 4 + [dma((6,))],
        compiler_params=pltpu.CompilerParams(
            collective_id=0, has_side_effects=True, vmem_limit_bytes=50 * 1024 * 1024),
        name="dispatch",
    )(moe_input, cotangent, routes_t, weights_t, gate_branch, states, out_proj)

    row_data = rows_in.reshape(groups * room, model)
    scaled = cot_in.reshape(groups * room, model)
    gate_w, up_w, down_w = w_gate[0], w_up[0], w_down[0]
    pre_gate = jnp.dot(row_data, gate_w, preferred_element_type=F32)
    pre_up = jnp.dot(row_data, up_w, preferred_element_type=F32)
    active, slope = silu_parts(pre_gate)
    hidden = (active * pre_up).astype(BF)
    grad_hidden = contract_cols(scaled, down_w)
    grad_pre_gate = (grad_hidden * pre_up * slope).astype(BF)
    grad_pre_up = (grad_hidden * active).astype(BF)
    entry_terms = (contract_cols(grad_pre_gate, gate_w) + contract_cols(grad_pre_up, up_w)).astype(BF)
    grad_down = contract_rows(hidden, scaled)
    grad_gate_w = contract_rows(row_data, grad_pre_gate)
    grad_up_w = contract_rows(row_data, grad_pre_up)

    grad_out_proj, grad_gate_branch, grad_log_decay, grad_input_term = pl.pallas_call(
        kernel_of(finish_kernel, "finish"),
        out_shape=[
            jax.ShapeDtypeStruct((high, chans), F32),
            jax.ShapeDtypeStruct((tok_rows, chans), BF),
            jax.ShapeDtypeStruct((tok_rows, chans), BF),
            jax.ShapeDtypeStruct((tok_rows, chans), F32),
        ],
        in_specs=[vmem] * 9,
        out_specs=[vmem] * 4,
        scratch_shapes=[
            pltpu.VMEM((parts - 1, groups, room, width), BF),
            pltpu.VMEM((groups, room, width), BF),
            pltpu.VMEM((groups, room, width), BF),
            pltpu.VMEM((model, tok_rows), BF),
            pltpu.VMEM((groups, high, tok_rows), BF),
            pltpu.VMEM((8, chans), F32),
            pltpu.VMEM((groups - 1, 8, chans), F32),
            pltpu.VMEM((8, chans), F32),
        ]
        + [dma((parts,))] * 2 + [dma((groups,))] * 2 + [dma((parts,))] * 2
        + [dma((groups,))] * 4 + [dma(())] * 2 + [dma((2,))],
        compiler_params=pltpu.CompilerParams(
            collective_id=1, has_side_effects=True, vmem_limit_bytes=50 * 1024 * 1024),
        name="finish",
    )(
        entry_terms.reshape(groups, room, model), cotangent, routes_t, weights_t, gate_branch,
        states, log_decay, proj_all.reshape(groups * high, chans), mixed_all,
    )
    return (
        grad_gate_w[None], grad_up_w[None], grad_down[None], grad_out_proj,
        grad_gate_branch, grad_log_decay, grad_input_term,
    )


def solution(mesh):
    return jax.shard_map(
        shards,
        mesh=mesh,
        in_specs=(
            P("sp", "tp"), P("sp", "tp"), P("sp", None), P("sp", None), P("sp", "tp"),
            P("sp", "tp"), P("sp", "tp"), P("sp", None, "tp"), P("sp", None, "tp"),
            P("sp", "tp", None), P("sp", "tp"),
        ),
        out_specs=(
            P("sp", None, "tp"), P("sp", None, "tp"), P("sp", "tp", None), P("sp", "tp"),
            P("sp", "tp"), P("sp", "tp"), P("sp", "tp"),
        ),
        check_vma=False,
    )
```

time: 256 us -> 140 us (0.55); the launches traced: 252 us -> 140 us
  Pallas kernels: 0 us -> 114 us
  blocking collectives: 69.8 us -> 0 us
  local copies, waits for them, and re-layouts: 68.4 us -> 10.9 us
  waiting for transfers between devices: 42.5 us -> 0 us
  other arithmetic: 18.7 us -> 0 us
  matrix products: 29.8 us -> 14.4 us
  between operations: 15.9 us -> 0.78 us
  starting transfers between devices: 7.14 us -> 0 us
    pallas_call x0 -> x2, Pallas kernels: none -> 114 us  [the longest x1 59.6 us: shards(): pl.pallas_call(kernel_of(dispatch_kernel, 'dispatch'), out_shape=[jax.Sha...]
    slice x52 -> x0, local copies, waits for them, and re-layouts: 42.4 us -> none  [the longest x49 40.8 us: shards(): lax.associative_scan(combine_pair, (jnp.flip(next_decay, 0), jnp.flip(gra...]
    all_gather x3 -> x0, blocking collectives: 38.2 us -> none  [the longest x2 27.9 us: carried_in(): pieces = jax.tree.map(lambda part: lax.all_gather(part, axis), value)]
    all_gather x3 -> x0, waiting for transfers between devices: 34.3 us -> none  [the longest x1 24.9 us: shards(): lax.all_gather(part_cot, 'tp', axis=2, tiled=True)]
    all_to_all x2 -> x0, blocking collectives: 31.6 us -> none  [the longest x1 17.4 us: shards(): lax.all_to_all(send_data.reshape(groups, room, col_width), 'sp', split_ax...]
    unnamed x54 -> x36, local copies, waits for them, and re-layouts: 2.52 us -> 10.9 us
    dot_general x3 -> x2, matrix products: 8.58 us -> 1.66 us  [the longest x1 0.83 us: shards(): pre_gate = jnp.dot(row_data, gate_w, preferred_element_type=F32)]
    mul x13 -> x0, other arithmetic: 6.02 us -> none  [the longest x12 5.2 us: combine_pair(): left_pair[0] * right_pair[0]]
  transfers between devices with their start and end apart: 7 -> 0, of which waited for: 4 -> 0; matrix products, arithmetic and copies ran while one was open for 40% -> 0% of each run, Pallas kernels for 0% -> 0%
where the time goes in v1:
time: 140 us
  Pallas kernels  114 us (81%)
  matrix products  14.4 us (10%)
  local copies, waits for them, and re-layouts  10.9 us (8%)
    pallas_call x1, Pallas kernels, shards(): pl.pallas_call(kernel_of(dispatch_kernel, 'dispatch'), out_shape=[jax.Sha...  59.6 us
    pallas_call x1, Pallas kernels, shards(): pl.pallas_call(kernel_of(finish_kernel, 'finish'), out_shape=[jax.ShapeDt...  54.2 us
    unnamed x36, local copies, waits for them, and re-layouts  10.9 us
    dot_general x3, matrix products, contract_rows(): lax.dot_general(left_mat, right_mat, (((0,), (0,)), ((), ())), preferred_...  9.96 us

profile of v1, /device:TPU:0, one launch (start us, length us, event | category | flops | bytes accessed | tf_op | source)
XLA Modules:
  0.0 139.8 jit_solution(329442618444702242)
XLA Ops:
  0.7 1.1 copy-done.1
  1.8 0.9 copy-done.3
  2.7 0.9 copy-done.5
  3.6 1.0 copy-done.8
  4.6 0.9 copy-done.9
  5.5 0.7 copy-done.10
  6.2 0.7 copy-done.12
  6.8 59.6 %dispatch.1 = (bf16[8,40,2048]{2,1,0:T(8,128)(2,1)S(1)}, bf16[8,40,2048]{2,1,0:T(8,128)(2,1)S(1)}, bf16[8,256,640]{2,1,0:T(8,128)(2,1)}, bf16[8,128,640]{2,1,0:T(8,128)(2,1)}) custom-call(bf16[128,512]{1,0:T(8,128)(2,1)S(1)} %copy-done.9, bf16[128,512]{1,0:T(8,128)(2,1)S(1)} %copy-done.5, s32[2,128]{1,0:T(2,128)S(1)} %bitcast.42, f32[2,128]{1,0:T(2,128)S(1)} %bitcast.44, ...), custom_call_target="tpu_custom_call" | custom-call | tf_op jit(solution)/shard_map/dispatch/pallas_call | solution.py:356
  66.4 0.8 fusion.3
  67.3 0.7 copy-done.14
  68.0 0.8 fusion.6
  68.8 0.8 copy-done.15
  69.6 1.0 multiply_convert_fusion.1
  70.7 3.4 %convolution_bitcast_fusion = f32[1,512,2048]{2,1,0:T(8,128)} fusion(bf16[320,2048]{1,0:T(8,128)(2,1)S(1)} %bitcast.47, f32[320,512]{1,0:T(8,128)S(1)} %fusion.6, f32[320,512]{1,0:T(8,128)S(1)} %fusion.3), kind=kOutput, calls=%fused_computation | convolution fusion | flops 672071680 | bytes 6815744 | tf_op jit(solution)/shard_map/dot_general | solution.py:21
  74.0 0.9 fusion.1
  75.0 0.9 fusion
  76.0 0.1 copy-done.7
  76.1 54.2 %finish.1 = (f32[256,640]{1,0:T(8,128)S(1)}, bf16[128,640]{1,0:T(8,128)(2,1)S(1)}, bf16[128,640]{1,0:T(8,128)(2,1)S(1)}, f32[128,640]{1,0:T(8,128)S(1)}) custom-call(bf16[8,40,2048]{2,1,0:T(8,128)(2,1)S(1)} %bitcast.41, bf16[128,512]{1,0:T(8,128)(2,1)S(1)} %copy-done.6, s32[2,128]{1,0:T(2,128)S(1)} %bitcast.43, f32[2,128]{1,0:T(2,128)S(1)} %bitcast.45, ...), custom_call_target="tpu_custom_call" | custom-call | tf_op jit(solution)/shard_map/finish/pallas_call | solution.py:390
  130.3 3.3 %convolution_bitcast_fusion.1 = f32[1,2048,512]{2,1,0:T(8,128)} fusion(bf16[320,2048]{1,0:T(8,128)(2,1)S(1)} %bitcast.39, bf16[320,512]{1,0:T(8,128)(2,1)S(1)} %get-tuple-element.23), kind=kOutput, calls=%fused_computation.1 | convolution fusion | flops 671088640 | bytes 5832704 | tf_op jit(solution)/shard_map/dot_general | solution.py:21
  133.6 3.3 %convolution_bitcast_fusion.2 = f32[1,2048,512]{2,1,0:T(8,128)} fusion(bf16[320,2048]{1,0:T(8,128)(2,1)S(1)} %bitcast.40, bf16[320,512]{1,0:T(8,128)(2,1)S(1)} %get-tuple-element.24), kind=kOutput, calls=%fused_computation.2 | convolution fusion | flops 671088640 | bytes 5832704 | tf_op jit(solution)/shard_map/dot_general | solution.py:21
  136.9 0.8 copy.22
  137.8 0.7 copy.23
  138.4 0.7 copy.24
  139.1 0.7 copy.25
  (22 shorter events, 0.2 us)
Async XLA Ops:
  0.6 65.8 %copy-start = (bf16[1,2048,512]{2,1,0:T(8,128)(2,1)S(1)}, bf16[1,2048,512]{2,1,0:T(8,128)(2,1)}, u32[]{:S(2)}) copy-start(bf16[1,2048,512]{2,1,0:T(8,128)(2,1)} %param.18) | copy-start | bytes 6291460
  0.6 1.1 copy-start.1
  1.8 0.9 copy-start.3
  2.7 0.9 copy-start.5
  3.6 1.0 copy-start.8
  4.6 0.9 copy-start.9
  5.5 0.7 copy-start.10
  6.2 0.7 copy-start.12
  66.4 1.6 %copy-start.14 = (bf16[1,2048,512]{2,1,0:T(8,128)(2,1)S(1)}, bf16[1,2048,512]{2,1,0:T(8,128)(2,1)}, u32[]{:S(2)}) copy-start(bf16[1,2048,512]{2,1,0:T(8,128)(2,1)} %param.19) | copy-start | bytes 6291460
  68.0 1.6 %copy-start.15 = (bf16[1,512,2048]{2,1,0:T(8,128)(2,1)S(1)}, bf16[1,512,2048]{2,1,0:T(8,128)(2,1)}, u32[]{:S(2)}) copy-start(bf16[1,512,2048]{2,1,0:T(8,128)(2,1)} %param.20) | copy-start | bytes 6291460
  74.9 1.0 copy-start.2
  74.9 1.0 copy-start.4
  74.9 1.1 copy-start.6
  74.9 1.2 copy-start.7
  74.9 1.2 copy-start.11
  74.9 1.2 copy-start.13

commit v2 on v1

v2 whole, which is shorter than its diff:
```python
import jax
import jax.numpy as jnp
from jax import lax
from jax.experimental import pallas as pl
from jax.experimental.pallas import tpu as pltpu
from jax.sharding import PartitionSpec as P

BF = jnp.bfloat16
F32 = jnp.float32
CORES = 2
GELU_C = 0.7978845608028654
GELU_A = 0.044715


def silu_parts(pre_gate):
    sigmoid_val = jax.nn.sigmoid(pre_gate)
    return (pre_gate * sigmoid_val, sigmoid_val * (1.0 + pre_gate * (1.0 - sigmoid_val)))


def contract_rows(left_mat, right_mat):
    return lax.dot_general(
        left_mat, right_mat, (((0,), (0,)), ((), ())), preferred_element_type=F32
    )


def contract_cols(left_mat, right_mat):
    return lax.dot_general(
        left_mat, right_mat, (((1,), (1,)), ((), ())), preferred_element_type=F32
    )


def gelu_parts(x):
    t = jnp.tanh(GELU_C * (x + GELU_A * (x * x * x)))
    half = 0.5 * (1.0 + t)
    slope = half + 0.5 * x * (1.0 - t * t) * (GELU_C * (1.0 + 3.0 * GELU_A * x * x))
    return x * half, slope


def selection(routes_t, weights_t, groups, room):
    picks, toks = routes_t.shape
    experts = lax.broadcasted_iota(jnp.int32, (groups, toks), 0)
    named = jnp.zeros((groups, toks), F32)
    weight = jnp.zeros((groups, toks), F32)
    for k in range(picks):
        hit = routes_t[k : k + 1, :] == experts
        named = named + jnp.where(hit, 1.0, 0.0)
        weight = weight + jnp.where(hit, weights_t[k : k + 1, :], 0.0)
    rows = lax.broadcasted_iota(jnp.int32, (toks, toks), 0)
    cols = lax.broadcasted_iota(jnp.int32, (toks, toks), 1)
    before = jnp.where(rows < cols, 1.0, 0.0).astype(BF)
    slot = jnp.dot(named.astype(BF), before, preferred_element_type=F32)
    slot = jnp.where(named > 0.5, slot, -1.0)
    place = lax.broadcasted_iota(jnp.int32, (room, toks), 0).astype(F32)
    picked, column = [], []
    for e in range(groups):
        one = jnp.where(slot[e : e + 1, :] == place, 1.0, 0.0)
        picked.append(one)
        column.append(jnp.sum(one * weight[e : e + 1, :], axis=1, keepdims=True))
    return jnp.concatenate(picked, axis=0).astype(BF), jnp.concatenate(column, axis=0)


def greet(groups, parts, mine, col):
    barrier = pltpu.get_barrier_semaphore()
    for d in range(1, groups):
        pl.semaphore_signal(
            barrier, inc=1, device_id={"sp": lax.rem(mine + d, groups)},
            device_id_type=pl.DeviceIdType.MESH,
        )
    for d in range(1, parts):
        pl.semaphore_signal(
            barrier, inc=1, device_id={"tp": lax.rem(col + d, parts)},
            device_id_type=pl.DeviceIdType.MESH,
        )
    pl.semaphore_wait(barrier, groups + parts - 2)


def remote(src, dst, send, recv, axis, peer):
    return pltpu.make_async_remote_copy(
        src_ref=src, dst_ref=dst, send_sem=send, recv_sem=recv,
        device_id={axis: peer}, device_id_type=pl.DeviceIdType.MESH,
    )


def whole_kernel(
    groups, parts, room, chunked,
    routes_ref, weights_ref, x_any, cot_any, gate_any, states_any, decay_any, proj_any,
    wg_any, wu_any, wd_any,
    gg_ref, gu_ref, gd_ref, outp_ref, ggate_ref, gdecay_ref, gin_ref,
    x_ref, cot_ref, gate_ref, states_ref, decay_ref, wg, wu, wd,
    out_x, out_c, rows_x, rows_c, proj_all, mixed_all, mix_own, gg, gu, gd,
    terms, shares, summed, back, flipped, blocks, carry_own, carry_in, prev_in,
    a_send, a_recv, t_send, t_recv, z_send, z_recv, c_send, c_recv,
    s_send, s_recv, r_send, r_recv, g_send, g_recv, b_send, b_recv, k_send, k_recv, p_send, p_recv,
    l_sem, w_sem,
):
    mine, col = lax.axis_index("sp"), lax.axis_index("tp")
    toks, width = x_ref.shape
    model = rows_x.shape[2]
    depth = groups // CORES
    z, core = mine // CORES, lax.rem(mine, CORES)
    size = groups * room

    def near(width_of, index):
        return pl.ds(pl.multiple_of(index * width_of, width_of), width_of)

    loads = []
    for i, (s, t) in enumerate((
        (x_any, x_ref), (cot_any, cot_ref), (gate_any, gate_ref), (states_any, states_ref),
        (proj_any, proj_all.at[mine]), (decay_any, decay_ref),
        (wg_any.at[0], wg), (wu_any.at[0], wu), (wd_any.at[0], wd),
    )):
        o = pltpu.make_async_copy(s, t, l_sem.at[i])
        o.start()
        loads.append(o)

    picked, weight = selection(routes_ref[...], weights_ref[...], groups, room)
    loads[0].wait()
    got = jnp.dot(picked, x_ref[...], preferred_element_type=F32).astype(BF)
    for e in range(groups):
        out_x[e] = got[e * room : (e + 1) * room]
    loads[1].wait()
    got_c = jnp.dot(picked, cot_ref[...], preferred_element_type=F32)
    got_c = (got_c * weight).astype(BF)
    for e in range(groups):
        out_c[e] = got_c[e * room : (e + 1) * room]
    greet(groups, parts, mine, col)

    here = near(width, col)
    sends, own = [], []
    arrivals = [[None] * groups for _ in range(2)]
    for a, (src, dst) in enumerate(((out_x, rows_x), (out_c, rows_c))):
        for d in range(1, groups):
            peer = lax.rem(mine + d, groups)
            c = remote(src.at[peer], dst.at[mine, :, here], a_send.at[a, d], a_recv.at[a, d], "sp", peer)
            c.start()
            arrivals[a][d] = c
            sends.append(c)
        o = pltpu.make_async_copy(src.at[mine], dst.at[mine, :, here], w_sem.at[a])
        o.start()
        own.append(o)

    pairs = (proj_all, mixed_all)

    def chain(a, step, wait=False):
        buf = pairs[a]
        right = buf.at[jnp.maximum(z - step, 0) * CORES + core]
        left = buf.at[jnp.minimum(z + step, depth - 1) * CORES + core]
        up = jnp.minimum(z + 1, depth - 1) * CORES + core
        down = jnp.maximum(z - 1, 0) * CORES + core
        for way, ref, peer, ok in (
            (0, right, up, jnp.logical_and(z - step >= 0, z + 1 < depth)),
            (1, left, down, jnp.logical_and(z + step < depth, z >= 1)),
        ):
            @pl.when(ok)
            def _(way=way, ref=ref, peer=peer):
                c = remote(ref, ref, z_send.at[a, way, step], z_recv.at[a, way, step], "sp", peer)
                c.wait_send() if wait else c.start()

    partner = z * CORES + (1 - core)

    def across(a, step, way, mode):
        ok = z - step >= 0 if way == 0 else z + step < depth
        zz = jnp.maximum(z - step, 0) if way == 0 else jnp.minimum(z + step, depth - 1)
        ref = pairs[a].at[zz * CORES + (1 - core if mode == "recv" else core)]

        @pl.when(ok)
        def _():
            c = remote(ref, ref, c_send.at[a, way, step], c_recv.at[a, way, step], "sp", partner)
            if mode == "start":
                c.start()
            elif mode == "send":
                c.wait_send()
            else:
                c.wait_recv()

    def advance(a, step):
        buf = pairs[a]
        from_l = buf.at[jnp.maximum(z - 1 - step, 0) * CORES + core]
        from_r = buf.at[jnp.minimum(z + 1 + step, depth - 1) * CORES + core]
        for way, ok, ref in ((0, z - 1 - step >= 0, from_l), (1, z + 1 + step < depth, from_r)):
            @pl.when(ok)
            def _(way=way, ref=ref):
                remote(ref, ref, z_send.at[a, way, step], z_recv.at[a, way, step],
                       "sp", lax.rem(mine + 1, groups)).wait_recv()
        if step + 1 < depth - 1:
            chain(a, step + 1)
        across(a, step + 1, 0, "start")
        across(a, step + 1, 1, "start")

    def settle(a):
        for step in range(depth - 1):
            chain(a, step, True)
        for step in range(depth):
            for way in range(2):
                if step or not way:
                    across(a, step, way, "send")

    def collected(a):
        for step in range(depth):
            for way in range(2):
                if step or not way:
                    across(a, step, way, "recv")

    loads[4].wait()
    chain(0, 0)
    across(0, 0, 0, "start")

    gathers = [[], []]

    def gather(a, src, dst):
        if chunked:
            for d in range(groups):
                at = lax.rem(mine + groups - d, groups)
                if d:
                    arrivals[a][d].wait_recv()
                for p in range(1, parts):
                    c = remote(dst.at[at, :, here] if d else src.at[mine], dst.at[at, :, here],
                               t_send.at[a, d, p], t_recv.at[a, d, p], "tp", lax.rem(col + p, parts))
                    c.start()
                    gathers[a].append(c)
            own[a].wait()
        else:
            own[a].wait()
            for d in range(1, groups):
                arrivals[a][d].wait_recv()
            for p in range(1, parts):
                c = remote(dst.at[:, :, here], dst.at[:, :, here],
                           t_send.at[a, 0, p], t_recv.at[a, 0, p], "tp", lax.rem(col + p, parts))
                c.start()
                gathers[a].append(c)
        sends.extend(gathers[a])

    gather(0, out_x, rows_x)
    loads[2].wait()
    loads[3].wait()
    act, branch_slope = gelu_parts(gate_ref[...].astype(F32))
    mix_own[...] = (act * states_ref[...]).astype(BF)
    gather(1, out_c, rows_c)
    o = pltpu.make_async_copy(mix_own, mixed_all.at[mine], w_sem.at[3])
    o.start()
    o.wait()
    for i in range(6, 9):
        loads[i].wait()
    for c in gathers[0]:
        c.wait_recv()
    row_data = rows_x[...].reshape(size, model)
    pre_gate = jnp.dot(row_data, wg[...], preferred_element_type=F32)
    pre_up = jnp.dot(row_data, wu[...], preferred_element_type=F32)
    active, slope = silu_parts(pre_gate)
    hidden = (active * pre_up).astype(BF)
    lean = pre_up * slope
    advance(0, 0)
    if depth > 2:
        advance(0, 1)
    for c in gathers[1]:
        c.wait_recv()
    grad_hidden = contract_cols(rows_c[...].reshape(size, model), wd[...])
    grad_pre_gate = (grad_hidden * lean).astype(BF)
    grad_pre_up = (grad_hidden * active).astype(BF)
    for d in list(range(1, parts)) + [0]:
        part = near(width, lax.rem(col + d, parts))
        term = contract_cols(grad_pre_gate, wg[part, :]) + contract_cols(grad_pre_up, wu[part, :])
        terms[d] = term.astype(BF).reshape(groups, room, width)

    share_copies = {}
    order = list(range(1, groups)) + [0]
    for d in order if chunked else [0]:
        at = lax.rem(mine + d, groups)
        for p in range(1, parts):
            src = terms.at[p, at] if chunked else terms.at[p]
            dst = shares.at[p - 1, at] if chunked else shares.at[p - 1]
            c = remote(src, dst, s_send.at[d, p], s_recv.at[d, p], "tp", lax.rem(col + p, parts))
            c.start()
            share_copies[d, p] = c
            sends.append(c)
    for step in range(2, depth - 1):
        advance(0, step)
    chain(1, 0)
    across(1, 0, 0, "start")

    stores = []

    def piece(kind, p):
        part = slice(p * width, (p + 1) * width)
        if kind == 2:
            gd[:, part] = contract_rows(hidden, rows_c[:, :, part].reshape(size, width)).astype(BF)
            s, t = gd.at[:, part], gd_ref.at[:, part]
        else:
            grad, buf, out = ((grad_pre_gate, gg, gg_ref), (grad_pre_up, gu, gu_ref))[kind]
            buf[part, :] = contract_rows(rows_x[:, :, part].reshape(size, width), grad).astype(BF)
            s, t = buf.at[part], out.at[part]
        o = pltpu.make_async_copy(s, t, w_sem.at[4 + kind * parts + p])
        o.start()
        stores.append(o)

    pieces = [(kind, p) for kind in range(3) for p in range(parts)]
    back_copies = []
    for d in order:
        if pieces:
            piece(*pieces.pop(0))
        at = lax.rem(mine + d, groups)
        if chunked or d == 1:
            for p in range(1, parts):
                share_copies[d if chunked else 0, p].wait_recv()
        total = terms[0, at].astype(F32)
        for p in range(1, parts):
            total = total + shares[p - 1, at].astype(F32)
        if d == 0:
            back[mine] = total.astype(BF)
        else:
            summed[d] = total.astype(BF)
            c = remote(summed.at[d], back.at[mine], r_send.at[d], r_recv.at[d], "sp", at)
            c.start()
            back_copies.append(c)
    nxt = lax.rem(mine + 1, groups)
    prev_copy = remote(states_ref.at[pl.ds(toks - 8, 8)], prev_in, p_send, p_recv, "sp", nxt)
    prev_copy.start()
    advance(1, 0)
    while pieces:
        piece(*pieces.pop(0))
    rows = lax.broadcasted_iota(jnp.int32, (toks, toks), 0)
    cols = lax.broadcasted_iota(jnp.int32, (toks, toks), 1)
    eye = jnp.where(rows == cols, 1.0, 0.0).astype(BF)
    total = contract_rows(cot_ref[...], eye)
    for c in back_copies:
        c.wait_recv()
    total = total + contract_rows(back[...].reshape(size, width), picked)
    flipped[here, :] = total.astype(BF)
    grad_copies = []
    for d in range(1, parts):
        part = flipped.at[here]
        c = remote(part, part, g_send.at[d], g_recv.at[d], "tp", lax.rem(col + d, parts))
        c.start()
        grad_copies.append(c)
    for step in range(1, depth - 1):
        advance(1, step)
    collected(0)
    loads[5].wait()
    for c in grad_copies:
        c.wait_recv()
    high = model // groups
    block_copies = []
    for d in range(1, groups):
        peer = lax.rem(mine + d, groups)
        c = remote(flipped.at[near(high, peer)], blocks.at[mine], b_send.at[d], b_recv.at[d], "sp", peer)
        c.start()
        block_copies.append(c)
    grad_mixed = contract_rows(flipped[...], proj_all[...].reshape(model, states_ref.shape[1]))
    states = states_ref[...]
    act, branch_slope = gelu_parts(gate_ref[...].astype(F32))
    decays = jnp.exp(decay_ref[...])
    ggate_ref[...] = (grad_mixed * states * branch_slope).astype(BF)
    local = grad_mixed * act
    line = lax.broadcasted_iota(jnp.int32, local.shape, 0)
    span = jnp.where(line < toks - 1, pltpu.roll(decays, toks - 1, 0), 1.0)
    k = 1
    while k < toks:
        inside = line < toks - k
        local = local + span * jnp.where(inside, pltpu.roll(local, toks - k, 0), 0.0)
        span = span * jnp.where(inside, pltpu.roll(span, toks - k, 0), 1.0)
        k *= 2
    eight = lax.broadcasted_iota(jnp.int32, (8, local.shape[1]), 0)
    whole = span[0:1] * decays[0:1]
    entry = local[0:1] * decays[0:1]
    carry_own[...] = jnp.where(eight == 0, whole, entry)
    carry_copies = []
    for d in range(1, groups):
        peer = lax.rem(mine + d, groups)
        c = remote(carry_own, carry_in.at[d - 1], k_send.at[d], k_recv.at[d], "sp", peer)
        c.start()
        carry_copies.append(c)
    collected(1)
    total = jnp.dot(flipped[near(high, mine), :], mixed_all[mine], preferred_element_type=F32)
    for d in range(1, groups):
        block_copies[d - 1].wait_recv()
        at = lax.rem(mine + groups - d, groups)
        total = total + jnp.dot(blocks[at], mixed_all[at], preferred_element_type=F32)
    outp_ref[...] = total
    prev_copy.wait_recv()
    first = jnp.where(mine > 0, prev_in[7:8, :], 0.0)
    prev = jnp.where(line == 0, first, pltpu.roll(states, 1, 0))
    for c in carry_copies:
        c.wait_recv()
    carried = jnp.zeros_like(whole)
    for ahead in range(groups - 1, 0, -1):
        got = carry_in[groups - ahead - 1]
        carried = jnp.where(mine + ahead < groups, got[1:2] + got[0:1] * carried, carried)
    grad_in = local + span * carried
    gin_ref[...] = grad_in
    gdecay_ref[...] = (grad_in * decays * prev).astype(BF)
    settle(0)
    settle(1)
    for c in [prev_copy] + sends + back_copies + grad_copies + block_copies + carry_copies:
        c.wait_send()
    for o in stores:
        o.wait()


def shards(
    moe_input, cotangent, routes, route_weights, gate_branch, log_decay, states,
    w_gate, w_up, w_down, out_proj,
):
    groups, parts = lax.axis_size("sp"), lax.axis_size("tp")
    tok_rows, picks = routes.shape
    width = moe_input.shape[1]
    model = width * parts
    units = w_gate.shape[2]
    chans = states.shape[1]
    room = tok_rows * picks * 5 // (4 * groups)
    room = (room + 7) // 8 * 8
    depth = groups // CORES
    high = out_proj.shape[0]
    chunked = groups * parts <= 64
    chunks = groups if chunked else 1
    vmem = pl.BlockSpec(memory_space=pltpu.VMEM)
    hbm = pl.BlockSpec(memory_space=pl.ANY)
    dma = pltpu.SemaphoreType.DMA

    def run(*refs):
        whole_kernel(groups, parts, room, chunked, *refs)

    def buf(*shape, kind=BF):
        return pltpu.VMEM(shape, kind)

    outs = pl.pallas_call(
        run,
        out_shape=[
            jax.ShapeDtypeStruct((model, units), BF),
            jax.ShapeDtypeStruct((model, units), BF),
            jax.ShapeDtypeStruct((units, model), BF),
            jax.ShapeDtypeStruct((high, chans), F32),
            jax.ShapeDtypeStruct((tok_rows, chans), BF),
            jax.ShapeDtypeStruct((tok_rows, chans), BF),
            jax.ShapeDtypeStruct((tok_rows, chans), F32),
        ],
        in_specs=[vmem] * 2 + [hbm] * 9,
        out_specs=[hbm] * 3 + [vmem] * 4,
        scratch_shapes=[
            buf(tok_rows, width), buf(tok_rows, width), buf(tok_rows, chans),
            buf(tok_rows, chans, kind=F32), buf(tok_rows, chans, kind=F32),
            buf(model, units), buf(model, units), buf(units, model),
            buf(groups, room, width), buf(groups, room, width),
            buf(groups, room, model), buf(groups, room, model),
            buf(groups, high, chans), buf(groups, tok_rows, chans), buf(tok_rows, chans),
            buf(model, units), buf(model, units), buf(units, model),
            buf(parts, groups, room, width), buf(parts - 1, groups, room, width),
            buf(groups, room, width), buf(groups, room, width),
            buf(model, tok_rows), buf(groups, high, tok_rows),
            buf(8, chans, kind=F32), buf(groups - 1, 8, chans, kind=F32), buf(8, chans, kind=F32),
        ]
        + [dma((2, groups))] * 2 + [dma((2, chunks, parts))] * 2 + [dma((2, 2, depth))] * 4
        + [dma((chunks, parts))] * 2 + [dma((groups,))] * 2 + [dma((parts,))] * 2
        + [dma((groups,))] * 4 + [dma(())] * 2 + [dma((9,)), dma((4 + 3 * parts,))],
        compiler_params=pltpu.CompilerParams(
            collective_id=0, has_side_effects=True, vmem_limit_bytes=60 * 1024 * 1024),
        name="backward",
    )(
        routes.T, route_weights.T, moe_input, cotangent, gate_branch, states, log_decay, out_proj,
        w_gate, w_up, w_down,
    )
    return tuple(out.astype(F32)[None] for out in outs[:3]) + tuple(outs[3:])


def solution(mesh):
    return jax.shard_map(
        shards,
        mesh=mesh,
        in_specs=(
            P("sp", "tp"), P("sp", "tp"), P("sp", None), P("sp", None), P("sp", "tp"),
            P("sp", "tp"), P("sp", "tp"), P("sp", None, "tp"), P("sp", None, "tp"),
            P("sp", "tp", None), P("sp", "tp"),
        ),
        out_specs=(
            P("sp", None, "tp"), P("sp", None, "tp"), P("sp", "tp", None), P("sp", "tp"),
            P("sp", "tp"), P("sp", "tp"), P("sp", "tp"),
        ),
        check_vma=False,
    )
```

time: 140 us -> 101 us (0.72)
  Pallas kernels: 114 us -> 87.7 us
  matrix products: 14.4 us -> 0 us
  other arithmetic: 0 us -> 9.51 us
  local copies, waits for them, and re-layouts: 10.9 us -> 2.91 us
    pallas_call x2 -> x1, Pallas kernels: 114 us -> 87.7 us  [shards(): pl.pallas_call(run, out_shape=[jax.ShapeDtypeStruct((model, units), BF),...]
    dot_general x8 -> x0, matrix products: 14.4 us -> none  [the longest x3 9.96 us: contract_rows(): lax.dot_general(left_mat, right_mat, (((0,), (0,)), ((), ())), preferred_...]
    broadcast_in_dim x0 -> x2, other arithmetic: none -> 9.51 us  [shards(): return tuple((out.astype(F32)[None] for out in outs[:3])) + tuple(outs[3:])]
    unnamed x36 -> x14, local copies, waits for them, and re-layouts: 10.9 us -> 2.91 us
where the time goes in v2:
time: 101 us
  Pallas kernels  87.7 us (87%)
  other arithmetic  9.51 us (9%)
  local copies, waits for them, and re-layouts  2.91 us (3%)
    pallas_call x1, Pallas kernels, shards(): pl.pallas_call(run, out_shape=[jax.ShapeDtypeStruct((model, units), BF),...  87.7 us
    broadcast_in_dim x2, other arithmetic, shards(): return tuple((out.astype(F32)[None] for out in outs[:3])) + tuple(outs[3:])  9.51 us
    unnamed x14, local copies, waits for them, and re-layouts  2.91 us

profile of v2, /device:TPU:0, one launch (start us, length us, event | category | flops | bytes accessed | tf_op | source)
XLA Modules:
  0.0 100.8 jit_solution(6210976582658520026)
XLA Ops:
  0.6 87.7 %backward.1 = (bf16[2048,512]{1,0:T(8,128)(2,1)}, bf16[2048,512]{1,0:T(8,128)(2,1)}, bf16[512,2048]{1,0:T(8,128)(2,1)}, f32[256,640]{1,0:T(8,128)}, bf16[128,640...) custom-call(s32[2,128]{1,0:T(2,128)} %bitcast.11, f32[2,128]{1,0:T(2,128)} %bitcast.12, ...), custom_call_target="tpu_custom_call" | custom-call | tf_op jit(solution)/shard_map/backward/pallas_call | solution.py:425
  88.3 0.0 copy-start
  88.3 7.0 %bitcast_convert_fusion.1 = (f32[1,2048,512]{2,1,0:T(8,128)}, f32[1,2048,512]{2,1,0:T(8,128)}) fusion(bf16[2048,512]{1,0:T(8,128)(2,1)} %get-tuple-element.15, bf16[2048,512]{1,0:T(8,128)(2,1)} %get-tuple-element.14), kind=kLoop, calls=%fused_computation.1 | loop fusion | flops 2097152 | bytes 12582912 | tf_op jit(solution)/shard_map/broadcast_in_dim | solution.py:461
  95.3 0.0 copy-done
  95.3 0.0 copy-start.1
  95.3 0.0 copy-start.4
  95.3 0.0 copy-start.3
  95.3 2.5 %bitcast_convert_fusion = f32[1,512,2048]{2,1,0:T(8,128)} fusion(bf16[512,2048]{1,0:T(8,128)(2,1)S(1)} %copy-done), kind=kLoop, calls=%fused_computation | loop fusion | flops 1048576 | bytes 6291456 | tf_op jit(solution)/shard_map/broadcast_in_dim | solution.py:461
  97.9 0.0 copy-start.2
  97.9 0.0 copy-done.1
  97.9 0.8 copy.22
  98.7 0.0 copy-done.4
  98.7 0.7 copy.23
  99.4 0.0 copy-done.3
  99.4 0.7 copy.24
  100.0 0.0 copy-done.2
  100.0 0.7 copy.25
Async XLA Ops:
  88.3 7.0 %copy-start = (bf16[512,2048]{1,0:T(8,128)(2,1)S(1)}, bf16[512,2048]{1,0:T(8,128)(2,1)}, u32[]{:S(2)}) copy-start(bf16[512,2048]{1,0:T(8,128)(2,1)} %get-tuple-element.16) | copy-start | bytes 6291460
  95.3 2.6 %copy-start.1 = (f32[256,640]{1,0:T(8,128)S(1)}, f32[256,640]{1,0:T(8,128)}, u32[]{:S(2)}) copy-start(f32[256,640]{1,0:T(8,128)} %get-tuple-element.33) | copy-start | bytes 1966084
  95.3 3.4 %copy-start.4 = (bf16[128,640]{1,0:T(8,128)(2,1)S(1)}, bf16[128,640]{1,0:T(8,128)(2,1)}, u32[]{:S(2)}) copy-start(bf16[128,640]{1,0:T(8,128)(2,1)} %get-tuple-element.34) | copy-start | bytes 491524
  95.3 4.1 %copy-start.3 = (bf16[128,640]{1,0:T(8,128)(2,1)S(1)}, bf16[128,640]{1,0:T(8,128)(2,1)}, u32[]{:S(2)}) copy-start(bf16[128,640]{1,0:T(8,128)(2,1)} %get-tuple-element.35) | copy-start | bytes 491524
  97.9 2.2 %copy-start.2 = (f32[128,640]{1,0:T(8,128)S(1)}, f32[128,640]{1,0:T(8,128)}, u32[]{:S(2)}) copy-start(f32[128,640]{1,0:T(8,128)} %get-tuple-element.36) | copy-start | bytes 983044
